TPU v7x, 32 devices: a whole 2x2x4 slice. The times are simulated.
32 devices in a mesh: sp: 4 (over z), fs: 4 (over y, x), tp: 2 (over core).
Axes of the slice: x: 2, y: 2, z: 4, core: 2. Of those that a mesh axis runs over, the one named last changes fastest.
Arguments:
- tokens: bfloat16 [4, 512, 4096], P('fs', 'sp'), may hold values from -6 to 6
- norm_gain: float32 [4096], replicated, may hold values from 0.1 to 1.9
- pool_proj: bfloat16 [4096, 1024], P(('sp', 'fs'), 'tp'), may hold values from -0.09375 to 0.09375
- query_proj: bfloat16 [4096, 1024], P(('sp', 'fs'), 'tp'), may hold values from -0.09375 to 0.09375
- key_proj: bfloat16 [4096, 1024], P(('sp', 'fs'), 'tp'), may hold values from -0.09375 to 0.09375
- value_proj: bfloat16 [4096, 1024], P(('sp', 'fs'), 'tp'), may hold values from -0.09375 to 0.09375
- pool_map: bfloat16 [4, 256, 256], replicated, may hold values from -0.375 to 0.375
- pool_scale: float32 [1024], replicated, may hold values from 0.1 to 1.9
- decay_rate: float32 [4], P('tp'), may hold values from 2e-05 to 0.034
- start_state: float32 [4, 4, 256, 256], P('fs', 'tp', 'sp'), may hold values from -96 to 96
- pool_back: bfloat16 [1024, 4096], P('tp', ('sp', 'fs')), may hold values from -0.125 to 0.125
- retention_back: bfloat16 [1024, 4096], P('tp', ('sp', 'fs')), may hold values from -0.125 to 0.125
Outputs:
- mixed: bfloat16 [4, 512, 4096], P('fs', ('sp', 'tp'))
All inputs are finite; a program needn't handle non-finite values.
Results may differ from a plain program's by a relative error of at most 0.014.
Values may be sent and summed in bfloat16 or wider, within the bound.
A program may use at most 128 MiB of HBM per device.

v0:
```python
import jax
import jax.numpy as jnp
from jax import lax
from jax.sharding import PartitionSpec as P

GROUPS = 4
BLOCK = 128
HALO = 16
eps = 1e-06
rope_base = 10000.0
highest_precision = lax.Precision.HIGHEST
window_list = (2, 4, 8, 16)


def shortened(x):
    return jax.tree.map(lambda a: a.astype(jnp.bfloat16) if a.dtype == jnp.float32 else a, x)


def shifted(x, axis, by):
    devices = lax.axis_size(axis)
    pairs = [(i, i + by) for i in range(devices) if 0 <= i + by < devices]
    return lax.ppermute(x, axis, pairs)


def carried_in(value, axis, join, neutral):
    count, mine = (lax.axis_size(axis), lax.axis_index(axis))
    pieces = jax.tree.map(lambda part: lax.all_gather(part, axis), value)
    running = jax.tree.map(
        lambda part, zero: jnp.full_like(part, 0) + jnp.asarray(zero, part.dtype), value, neutral
    )

    def turn(position, running):
        longer = join(running, jax.tree.map(lambda part: part[position], pieces))
        return jax.tree.map(lambda new, old: jnp.where(position < mine, new, old), longer, running)

    return lax.fori_loop(0, count - 1, turn, running)


def rotate(values, positions):
    half_dim = values.shape[-1] // 2
    inv_freq = 1.0 / rope_base ** jnp.linspace(0.0, 1.0, half_dim, dtype=jnp.float32)
    angles = positions.astype(jnp.float32)[:, None] * inv_freq[None, :]
    cosine = jnp.cos(angles)[:, None, :]
    sine = jnp.sin(angles)[:, None, :]
    first_half = values[..., :half_dim]
    second_half = values[..., half_dim:]
    return jnp.concatenate(
        [first_half * cosine - second_half * sine, first_half * sine + second_half * cosine],
        axis=-1,
    )


def trailing_sums(extended, length):
    begin = extended.shape[0] - length
    running = extended[begin:]
    results = []
    for behind in range(1, 16):
        running = running + extended[begin - behind : begin - behind + length]
        if behind + 1 in window_list:
            results.append(running)
    return results


def reshape_blocks(array):
    return array.reshape((array.shape[0] // BLOCK, BLOCK) + array.shape[1:])


def block_retention(queries, keys_in, values_in, decay_rate, initial):
    length, head_count, head_dim = queries.shape
    within = jnp.arange(BLOCK, dtype=jnp.float32)
    distance = within[:, None] - within[None, :]
    decay_mask = jnp.where(
        distance[None] >= 0,
        jnp.exp(-jnp.maximum(distance, 0.0)[None] * decay_rate[:, None, None]),
        0.0,
    )
    query_decay_factor = jnp.exp(-(within + 1.0)[:, None] * decay_rate[None, :])
    key_decay_factor = jnp.exp(-(BLOCK - 1.0 - within)[:, None] * decay_rate[None, :])
    block_decay_factor = jnp.exp(-BLOCK * decay_rate)

    def advance(state_carry, inputs):
        block_queries, block_keys, block_values = inputs
        scores = (
            jnp.einsum("ihk,jhk->hij", block_queries, block_keys, precision=highest_precision)
            * decay_mask
        )
        inside = jnp.einsum("hij,jhv->ihv", scores, block_values, precision=highest_precision)
        across_blocks = jnp.einsum(
            "bzy,zyx->bzx",
            block_queries * query_decay_factor[:, :, None],
            state_carry,
            precision=highest_precision,
        )
        state_carry = state_carry * block_decay_factor[:, None, None] + jnp.einsum(
            "flm,fld->lmd",
            block_keys * key_decay_factor[:, :, None],
            block_values,
            precision=highest_precision,
        )
        return (state_carry, inside + across_blocks)

    final_state, outputs = lax.scan(
        advance,
        initial,
        (reshape_blocks(queries), reshape_blocks(keys_in), reshape_blocks(values_in)),
    )
    return (outputs.reshape(length, head_count, values_in.shape[-1]), final_state)


def combine_states(earlier, latter):
    return (earlier[0] * latter[0], latter[0][:, None, None] * earlier[1] + latter[1])


def on_device(
    tokens,
    norm_gain,
    pool_proj,
    query_proj,
    key_proj,
    value_proj,
    pool_map,
    pool_scale,
    decay_rate,
    start_state,
    pool_back,
    retention_back,
):
    sequence = tokens[0]
    length = sequence.shape[0]
    tp_index = lax.axis_index("tp")
    sp_index = lax.axis_index("sp")
    tp_count = lax.axis_size("tp")
    floats = sequence.astype(jnp.float32)
    normed = (
        floats * lax.rsqrt(jnp.mean(floats * floats, axis=-1, keepdims=True) + eps) * norm_gain
    ).astype(jnp.bfloat16)
    group_normed = lax.all_gather(normed, "fs", axis=0, tiled=True)
    quarters = (
        lax.all_to_all(pool_proj, "fs", split_axis=1, concat_axis=0, tiled=True),
        lax.all_to_all(query_proj, "fs", split_axis=1, concat_axis=0, tiled=True),
        lax.all_to_all(key_proj, "fs", split_axis=1, concat_axis=0, tiled=True),
        lax.all_to_all(value_proj, "fs", split_axis=1, concat_axis=0, tiled=True),
    )
    pieces = (
        lax.all_gather(quarters[0], "sp", axis=0, tiled=True),
        lax.all_gather(quarters[1], "sp", axis=0, tiled=True),
        lax.all_gather(quarters[2], "sp", axis=0, tiled=True),
        lax.all_gather(quarters[3], "sp", axis=0, tiled=True),
    )
    partial_cols = tuple(
        (jnp.dot(group_normed, piece_w, preferred_element_type=jnp.float32) for piece_w in pieces)
    )
    rounded = tuple((result.astype(jnp.bfloat16) for result in partial_cols))
    pool_in, query_bf, key_bf, value_bf = jax.tree.map(
        lambda part, own: part.astype(own.dtype),
        lax.all_to_all(shortened(rounded), "fs", split_axis=0, concat_axis=1, tiled=True),
        rounded,
    )
    positions = jnp.arange(length, dtype=jnp.int32) + sp_index * length
    before = shifted(pool_in[length - HALO :], "sp", 1)
    extended = jnp.concatenate([before, pool_in], axis=0).astype(jnp.float32)
    stacked = jnp.stack(trailing_sums(extended, length))
    local_groups = GROUPS // tp_count
    channels = pool_in.shape[1]
    group_dim = channels // local_groups
    group_maps = lax.dynamic_slice_in_dim(pool_map, tp_index * local_groups, local_groups, 0)
    scales = lax.dynamic_slice_in_dim(pool_scale, tp_index * channels, channels, 0)
    windows = jnp.array(window_list, dtype=jnp.int32)
    pieces = []
    for group_idx in range(local_groups):
        chosen_group = tp_index * local_groups + group_idx
        lower = group_idx * group_dim
        chosen = lax.dynamic_index_in_dim(stacked, chosen_group, 0, keepdims=False)[
            :, lower : lower + group_dim
        ]
        counts = jnp.minimum(windows[chosen_group], positions + 1).astype(jnp.float32)
        inputs = extended[HALO:, lower : lower + group_dim]
        differ = (chosen / counts[:, None] - inputs).astype(jnp.bfloat16)
        pieces.append(jnp.dot(differ, group_maps[group_idx], preferred_element_type=jnp.float32))
    pool_out = (jnp.concatenate(pieces, axis=1) * scales).astype(jnp.bfloat16)
    head_count = decay_rate.shape[0]
    head_dim = query_bf.shape[1] // head_count
    queries = rotate(query_bf.astype(jnp.float32).reshape(length, head_count, head_dim), positions)
    keys_in = rotate(
        key_bf.astype(jnp.float32).reshape(length, head_count, head_dim), positions
    ) * head_dim ** (-0.5)
    values_in = value_bf.astype(jnp.float32).reshape(length, head_count, head_dim)
    zeros_state = jnp.zeros((head_count, head_dim, head_dim), jnp.float32)
    local_output, local_state = block_retention(
        queries, keys_in, values_in, decay_rate, zeros_state
    )
    span_decay = jnp.exp(-decay_rate * length)
    whole_start = lax.all_gather(start_state, "sp", axis=2, tiled=True)[0]
    span_factor, carried_over = carried_in(
        (span_decay, local_state), "sp", combine_states, (jnp.ones_like(span_decay), zeros_state)
    )
    offset_float = (sp_index * length).astype(jnp.float32)
    carried_over = carried_over + jnp.exp(-decay_rate * offset_float)[:, None, None] * whole_start
    steps_in = jnp.arange(length, dtype=jnp.float32) + 1.0
    query_rows_scaled = queries * jnp.exp(-steps_in[:, None] * decay_rate[None, :])[:, :, None]
    retained_output = local_output + jnp.einsum(
        "lpi,pib->lpb", query_rows_scaled, carried_over, precision=highest_precision
    )
    retained_output = retained_output * lax.rsqrt(
        jnp.mean(retained_output * retained_output, axis=-1, keepdims=True) + eps
    )
    ret_out = retained_output.reshape(length, head_count * head_dim).astype(jnp.bfloat16)
    pool_cols, retention_cols = (
        lax.all_gather(pool_back, ("sp", "fs"), axis=1, tiled=True),
        lax.all_gather(retention_back, ("sp", "fs"), axis=1, tiled=True),
    )
    weight_local = jnp.concatenate([pool_cols, retention_cols], axis=0)
    joined = jnp.concatenate([pool_out, ret_out], axis=1)
    mixed = lax.psum_scatter(
        jnp.dot(joined, weight_local, preferred_element_type=jnp.float32).astype(jnp.bfloat16),
        "tp",
        scatter_dimension=0,
        tiled=True,
    )
    return mixed[None]


def solution(mesh):
    placed = (
        P("fs", "sp", None),
        P(),
        P(("sp", "fs"), "tp"),
        P(("sp", "fs"), "tp"),
        P(("sp", "fs"), "tp"),
        P(("sp", "fs"), "tp"),
        P(),
        P(),
        P("tp"),
        P("fs", "tp", "sp", None),
        P("tp", ("sp", "fs")),
        P("tp", ("sp", "fs")),
    )
    return jax.shard_map(
        on_device,
        mesh=mesh,
        in_specs=placed,
        out_specs=P("fs", ("sp", "tp"), None),
        check_vma=False,
    )
```

profile of v0, /device:TPU:0, one launch (start us, length us, event | category | flops | bytes accessed | tf_op | source)
XLA Modules:
  0.0 432.0 jit_solution(100196734017617633)
XLA Ops:
  7.7 10.7 %all_to_all.137 = bf16[256,4,128]{0,2,1:T(8,128)(2,1)S(1)} all-to-all(bf16[256,4,128]{0,2,1:T(8,128)(2,1)S(1)} %bitcast.100), channel_id=1, replica_groups=mesh['sp'=4,'fs'=4,'tp'=2] {'fs'}, dimensions={1} | all-to-all | bytes 524288 | tf_op jit(solution)/shard_map/all_to_all | solution.py:140
  23.7 8.1 %all_to_all.138 = bf16[256,4,128]{0,2,1:T(8,128)(2,1)S(1)} all-to-all(bf16[256,4,128]{0,2,1:T(8,128)(2,1)S(1)} %bitcast.101), channel_id=1, replica_groups=mesh['sp'=4,'fs'=4,'tp'=2] {'fs'}, dimensions={1} | all-to-all | bytes 524288 | tf_op jit(solution)/shard_map/all_to_all | solution.py:141
  32.9 8.1 %all_to_all.139 = bf16[256,4,128]{0,2,1:T(8,128)(2,1)S(1)} all-to-all(bf16[256,4,128]{0,2,1:T(8,128)(2,1)S(1)} %bitcast.102), channel_id=1, replica_groups=mesh['sp'=4,'fs'=4,'tp'=2] {'fs'}, dimensions={1} | all-to-all | bytes 524288 | tf_op jit(solution)/shard_map/all_to_all | solution.py:142
  42.8 3.4 all-to-all-start
  48.0 3.5 all-to-all-done
  52.4 48.6 %all-gather.11.cloned.1.call-done = bf16[512,4096]{1,0:T(8,128)(2,1)} async-done(((bf16[128,4096]{1,0:T(8,128)(2,1)}), bf16[512,4096]{1,0:T(8,128)(2,1)}) %all-gather.11.cloned.1.call-update) | async-done | bytes 4194320 | tf_op jit(solution)/shard_map/all_gather | solution.py:137
  101.0 3.7 convolution_convert_fusion.1
  108.8 21.8 %all-gather.19.cloned.1.call-done = bf16[4096,128]{1,0:T(8,128)(2,1)} async-done(((bf16[1024,128]{1,0:T(8,128)(2,1)}), bf16[4096,128]{1,0:T(8,128)(2,1)}) %all-gather.19.cloned.1.call-update) | async-done | bytes 1048592 | tf_op jit(solution)/shard_map/all_gather | solution.py:147
  130.6 3.7 convolution_convert_fusion
  135.1 3.7 all-to-all-start.7
  138.7 20.7 %all-gather.15.cloned.1.call-done = bf16[4096,128]{1,0:T(8,128)(2,1)} async-done(((bf16[1024,128]{1,0:T(8,128)(2,1)}), bf16[4096,128]{1,0:T(8,128)(2,1)}) %all-gather.15.cloned.1.call-update) | async-done | bytes 1048592 | tf_op jit(solution)/shard_map/all_gather | solution.py:148
  159.4 4.4 %convolution_convert_fusion.2 = bf16[512,128]{1,0:T(8,128)(2,1)} fusion(bf16[512,4096]{1,0:T(8,128)(2,1)} %all-gather.11.cloned.1.call-done, bf16[4096,128]{1,0:T(8,128)(2,1)} %all-gather.15.cloned.1.call-done), kind=kOutput, calls=%fused_computation.19 | convolution fusion | flops 536936448 | bytes 5373952 | tf_op jit(solution)/shard_map/dot_general | solution.py:151
  163.8 3.8 all-to-all-start.3
  168.1 4.5 %all-to-all-done.3 = bf16[4,128,128]{2,1,0:T(8,128)(2,1)S(1)} async-done(((bf16[4,128,128]{2,1,0:T(8,128)(2,1)}), bf16[4,128,128]{2,1,0:T(8,128)(2,1)S(1)}, u32[]{:S(2)}, u32[]{:S(2)}) %all-to-all-start.3) | async-done | bytes 131104 | tf_op jit(solution)/shard_map/all_to_all | solution.py:156
  175.7 10.7 %all-reduce = f32[8]{0:T(128)S(1)} all-reduce(f32[8]{0:T(128)S(1)} %get-tuple-element.181), channel_id=2, replica_groups=mesh['sp'=4,'fs'=4,'tp'=2] {'sp'}, use_global_device_ids=true, to_apply=%add | all-reduce | flops 8 | bytes 64
  187.2 14.7 %all_gather.45 = f32[1,2,256,256]{3,2,1,0:T(8,128)S(1)} all-gather(f32[1,2,64,256]{3,2,1,0:T(8,128)S(1)} %copy-done.4), channel_id=1, replica_groups=mesh['sp'=4,'fs'=4,'tp'=2] {'sp'}, dimensions={2}, use_global_device_ids=true | all-gather | bytes 655360 | tf_op jit(solution)/shard_map/all_gather | solution.py:193
  201.9 3.7 convolution_convert_fusion.3
  211.1 3.7 all-to-all-done.1
  221.7 14.9 %all-gather.25.cloned.1.call-done = f32[8,256,256]{2,1,0:T(8,128)} async-done(((f32[2,256,256]{2,1,0:T(8,128)}), f32[8,256,256]{2,1,0:T(8,128)}) %all-gather.25.cloned.1.call-update) | async-done | bytes 2097168 | tf_op jit(solution)/shard_map/all_gather | solution.py:27
  236.6 3.6 while.9
  241.5 83.7 %all-gather.21.cloned.1.call-done = bf16[512,4096]{1,0:T(8,128)(2,1)} async-done(((bf16[512,256]{1,0:T(8,128)(2,1)}), bf16[512,4096]{1,0:T(8,128)(2,1)}) %all-gather.21.cloned.1.call-update) | async-done | bytes 4194320 | tf_op jit(solution)/shard_map/all_gather | solution.py:209
  325.2 87.7 %all-gather.23.cloned.1.call-done = bf16[512,4096]{1,0:T(8,128)(2,1)} async-done(((bf16[512,256]{1,0:T(8,128)(2,1)}), bf16[512,4096]{1,0:T(8,128)(2,1)}) %all-gather.23.cloned.1.call-update) | async-done | bytes 4194320 | tf_op jit(solution)/shard_map/all_gather | solution.py:210
  412.9 5.8 %fusion.5 = bf16[128,4096]{1,0:T(8,128)(2,1)} fusion(bf16[512,4096]{1,0:T(8,128)(2,1)} %all-gather.23.cloned.1.call-done, bf16[512,4096]{1,0:T(8,128)(2,1)} %all-gather.21.cloned.1.call-done, bf16[128,512]{1,0:T(8,128)(2,1)S(1)} %copy.76, bf16[128,512]{1,0:T(8,128)(2,1)S(1)} %fusion.15), kind=kOutput, calls=%fused_computation.7 | convolution fusion | flops 1091567616 | bytes 9699328 | tf_op jit(solution)/shard_map/dot_general | solution.py:215
  418.8 6.7 %reduce-scatter.2.cloned.1.call-done = bf16[64,4096]{1,0:T(8,128)(2,1)} async-done(((bf16[128,4096]{1,0:T(8,128)(2,1)}), bf16[64,4096]{1,0:T(8,128)(2,1)}) %reduce-scatter.2.cloned.1.call-update) | async-done | bytes 524304 | tf_op jit(solution)/shard_map/reduce_scatter | solution.py:214
  (108 shorter events, 37.6 us)
Async XLA Ops:
  6.5 214.6 %copy-start = (bf16[4,256,256]{2,1,0:T(8,128)(2,1)S(1)}, bf16[4,256,256]{2,1,0:T(8,128)(2,1)}, u32[]{:S(2)}) copy-start(bf16[4,256,256]{2,1,0:T(8,128)(2,1)} %param.23) | copy-start | bytes 1572868
  6.5 17.1 %copy-start.1 = (bf16[256,512]{1,0:T(8,128)(2,1)S(1)}, bf16[256,512]{1,0:T(8,128)(2,1)}, u32[]{:S(2)}) copy-start(bf16[256,512]{1,0:T(8,128)(2,1)} %param.21) | copy-start | bytes 786436
  6.5 26.2 %copy-start.2 = (bf16[256,512]{1,0:T(8,128)(2,1)S(1)}, bf16[256,512]{1,0:T(8,128)(2,1)}, u32[]{:S(2)}) copy-start(bf16[256,512]{1,0:T(8,128)(2,1)} %param.22) | copy-start | bytes 786436
  6.5 45.9 %all-gather.17.cloned.1.call-start = ((), (), s32[]{:S(2)}) async-start(), calls=%async_computation.12 | async-start | bytes 1310720 | tf_op jit(solution)/shard_map/all_gather | solution.py:146
  19.3 22.6 %copy-start.3 = (bf16[256,512]{1,0:T(8,128)(2,1)S(1)}, bf16[256,512]{1,0:T(8,128)(2,1)}, u32[]{:S(2)}) copy-start(bf16[256,512]{1,0:T(8,128)(2,1)} %param.19) | copy-start | bytes 786436
  19.3 81.7 %all-gather.11.cloned.1.call-start = ((), (), s32[]{:S(2)}) async-start(), calls=%async_computation.9 | async-start | bytes 5242880 | tf_op jit(solution)/shard_map/all_gather | solution.py:137
  20.9 25.3 %copy-start.8 = (u32[32]{0:T(128)S(1)}, u32[32]{0:T(128)}, u32[]{:S(2)}) copy-start(u32[32]{0:T(128)} %constant.104) | copy-start | bytes 388
  20.9 26.6 %copy-start.5 = (f32[2]{0:T(128)S(1)}, f32[2]{0:T(128)}, u32[]{:S(2)}) copy-start(f32[2]{0:T(128)} %param.25) | copy-start | bytes 28
  23.5 107.0 %all-gather.19.cloned.1.call-start = ((), (), s32[]{:S(2)}) async-start(), calls=%async_computation.13 | async-start | bytes 1310720 | tf_op jit(solution)/shard_map/all_gather | solution.py:147
  32.7 126.7 %all-gather.15.cloned.1.call-start = ((), (), s32[]{:S(2)}) async-start(), calls=%async_computation.11 | async-start | bytes 1310720 | tf_op jit(solution)/shard_map/all_gather | solution.py:148
  42.8 8.8 %all-to-all-start = ((bf16[256,4,128]{0,2,1:T(8,128)(2,1)}), bf16[256,4,128]{0,2,1:T(8,128)(2,1)S(1)}, u32[]{:S(2)}, u32[]{:S(2)}) async-start(bf16[256,4,128]{0,2,1:T(8,128)(2,1)} %bitcast.2), calls=%async_computation | async-start | bytes 524288 | tf_op jit(solution)/shard_map/all_to_all | solution.py:139
  46.2 155.7 %all-gather.13.cloned.1.call-start = ((), (), s32[]{:S(2)}) async-start(), calls=%async_computation.10 | async-start | bytes 1310720 | tf_op jit(solution)/shard_map/all_gather | solution.py:145
  105.5 29.6 %all-to-all-start.5 = ((bf16[4,128,128]{1,2,0:T(8,128)(2,1)}), bf16[4,128,128]{1,2,0:T(8,128)(2,1)S(1)}, u32[]{:S(2)}, u32[]{:S(2)}) async-start(bf16[4,128,128]{1,2,0:T(8,128)(2,1)} %copy.60), calls=%async_computation.5 | async-start | bytes 262144 | tf_op jit(solution)/shard_map/all_to_all | solution.py:156
  135.1 28.7 %all-to-all-start.7 = ((bf16[4,128,128]{1,2,0:T(8,128)(2,1)}), bf16[4,128,128]{1,2,0:T(8,128)(2,1)S(1)}, u32[]{:S(2)}, u32[]{:S(2)}) async-start(bf16[4,128,128]{1,2,0:T(8,128)(2,1)} %copy.65), calls=%async_computation.7 | async-start | bytes 262144 | tf_op jit(solution)/shard_map/all_to_all | solution.py:156
  163.8 22.6 %copy-start.7 = (f32[1024]{0:T(1024)S(1)}, f32[1024]{0:T(1024)}, u32[]{:S(2)}) copy-start(f32[1024]{0:T(1024)} %param.24) | copy-start | bytes 12292
  163.8 22.7 %copy-start.6 = (s32[4]{0:T(128)S(1)}, s32[4]{0:T(128)}, u32[]{:S(2)}) copy-start(s32[4]{0:T(128)} %constant.99.clone) | copy-start | bytes 52
  163.8 23.4 %copy-start.4 = (f32[1,2,64,256]{3,2,1,0:T(8,128)S(1)}, f32[1,2,64,256]{3,2,1,0:T(8,128)}, u32[]{:S(2)}) copy-start(f32[1,2,64,256]{3,2,1,0:T(8,128)} %param.26) | copy-start | bytes 393220
  163.8 8.8 %all-to-all-start.3 = ((bf16[4,128,128]{2,1,0:T(8,128)(2,1)}), bf16[4,128,128]{2,1,0:T(8,128)(2,1)S(1)}, u32[]{:S(2)}, u32[]{:S(2)}) async-start(bf16[4,128,128]{2,1,0:T(8,128)(2,1)} %bitcast.22), calls=%async_computation.3 | async-start | bytes 262144 | tf_op jit(solution)/shard_map/all_to_all | solution.py:156
  167.6 69.0 %all-gather.25.cloned.1.call-start = ((), (), s32[]{:S(2)}) async-start(), calls=%async_computation.17 | async-start | bytes 2621440 | tf_op jit(solution)/shard_map/all_gather | solution.py:27
  174.2 151.0 %all-gather.21.cloned.1.call-start = ((), (), s32[]{:S(2)}) async-start(), calls=%async_computation.14 | async-start | bytes 4456448 | tf_op jit(solution)/shard_map/all_gather | solution.py:209
  174.9 238.0 %all-gather.23.cloned.1.call-start = ((), (), s32[]{:S(2)}) async-start(), calls=%async_computation.15 | async-start | bytes 4456448 | tf_op jit(solution)/shard_map/all_gather | solution.py:210
  206.4 8.3 %all-to-all-start.1 = ((bf16[4,128,128]{1,2,0:T(8,128)(2,1)}), bf16[4,128,128]{1,2,0:T(8,128)(2,1)S(1)}, u32[]{:S(2)}, u32[]{:S(2)}) async-start(bf16[4,128,128]{1,2,0:T(8,128)(2,1)} %copy.52), calls=%async_computation.1 | async-start | bytes 262144 | tf_op jit(solution)/shard_map/all_to_all | solution.py:156
  209.7 215.7 %reduce-scatter.2.cloned.1.call-start = ((), (), s32[]{:S(2)}) async-start(), calls=%async_computation.16 | async-start | bytes 1572864 | tf_op jit(solution)/shard_map/reduce_scatter | solution.py:214
  214.9 4.6 %collective-permute-start = (bf16[16,512]{1,0:T(8,128)(2,1)S(1)}, bf16[16,512]{1,0:T(8,128)(2,1)S(1)}, u32[]{:S(2)}, u32[]{:S(2)}) collective-permute-start(bf16[16,512]{1,0:T(8,128)(2,1)S(1)} %copy.75), channel_id=1, source_target_pairs={{0,8},{8,16},{16,24},{1,9},{9,17},{17,25},{2,10},{10,18},{18,26},{... | collective-permute-start | bytes 49160 | tf_op jit(solution)/shard_map/ppermute | solution.py:22
Sparse Core Ops, SparseCore 0:
  19.4 27.6 all-gather.16
  49.0 51.9 all-gather.10
  102.6 27.9 all-gather.18
  132.0 27.3 all-gather.14
  160.8 28.7 all-gather.12
  191.1 45.4 all-gather.24
  239.3 85.8 all-gather.20
  327.9 84.9 all-gather.22
  418.9 6.5 reduce-scatter.1
where the time goes:
time: 433 us; the launch traced here: 432 us
  waiting for transfers between devices  297 us (69%)
  blocking collectives  52.3 us (12%)
  matrix products  25.7 us (6%)
  starting transfers between devices  20.9 us (5%)
  between operations  14.2 us (3%)
  other arithmetic  11.1 us (3%)
  local copies, waits for them, and re-layouts  10.4 us (2%)
    all_gather x1, waiting for transfers between devices, on_device(): lax.all_gather(retention_back, ('sp', 'fs'), axis=1, tiled=True)  87.7 us
    all_gather x1, waiting for transfers between devices, on_device(): lax.all_gather(pool_back, ('sp', 'fs'), axis=1, tiled=True)  83.7 us
    all_gather x1, waiting for transfers between devices, on_device(): group_normed = lax.all_gather(normed, 'fs', axis=0, tiled=True)  48.6 us
    all_gather x1, waiting for transfers between devices, on_device(): lax.all_gather(quarters[2], 'sp', axis=0, tiled=True)  21.8 us
    all_gather x1, waiting for transfers between devices, on_device(): lax.all_gather(quarters[3], 'sp', axis=0, tiled=True)  20.7 us
    dot_general x4, matrix products, on_device(): jnp.dot(group_normed, piece_w, preferred_element_type=jnp.float32)  15.6 us
    all_gather x1, waiting for transfers between devices, carried_in(): pieces = jax.tree.map(lambda part: lax.all_gather(part, axis), value)  14.9 us
    all_gather x1, blocking collectives, on_device(): whole_start = lax.all_gather(start_state, 'sp', axis=2, tiled=True)[0]  14.7 us
  transfers between devices with their start and end apart: 15, of which 11 were waited for; matrix products, arithmetic and copies ran while one was open for 9% of the time, Pallas kernels for 0%

commit v1 on v0

--- a/solution.py
+++ b/solution.py
@@ -207,7 +207,7 @@
     ret_out = retained_output.reshape(length, head_count * head_dim).astype(jnp.bfloat16)
     pool_cols, retention_cols = (
         lax.all_gather(pool_back, ("sp", "fs"), axis=1, tiled=True),
-        lax.all_gather(retention_back, ("sp", "fs"), axis=1, tiled=True),
+        jnp.concatenate(lax.all_gather(retention_back, ("sp", "fs")), axis=1),
     )
     weight_local = jnp.concatenate([pool_cols, retention_cols], axis=0)
     joined = jnp.concatenate([pool_out, ret_out], axis=1)

time: 433 us -> 423 us (0.977)
  waiting for transfers between devices: 297 us -> 279 us
  blocking collectives: 52.3 us -> 60.6 us
  starting transfers between devices: 20.9 us -> 15.9 us
    all_gather x1, waiting for transfers between devices: 87.7 us -> 48.7 us  [on_device(): lax.all_gather(retention_back, ('sp', 'fs'))]
    all_gather x1, waiting for transfers between devices: 14.9 us -> 41.1 us  [carried_in(): pieces = jax.tree.map(lambda part: lax.all_gather(part, axis), value)]
    all_to_all x0 -> x1, blocking collectives: none -> 8.11 us  [on_device(): lax.all_to_all(pool_proj, 'fs', split_axis=1, concat_axis=0, tiled=True)]
    reshape x0 -> x1, local copies, waits for them, and re-layouts: none -> 4.76 us  [on_device(): jnp.concatenate(lax.all_gather(retention_back, ('sp', 'fs')), axis=1)]
  transfers between devices with their start and end apart: 15 -> 14, of which waited for: 11 -> 9; matrix products, arithmetic and copies ran while one was open for 9% -> 10% of each run, Pallas kernels for 0% -> 0%
where the time goes in v1:
time: 423 us; the launch traced here: 422 us
  waiting for transfers between devices  279 us (66%)
  blocking collectives  60.6 us (14%)
  matrix products  25.8 us (6%)
  starting transfers between devices  15.9 us (4%)
  local copies, waits for them, and re-layouts  14.6 us (3%)
  between operations  14.3 us (3%)
  other arithmetic  11.1 us (3%)
    all_gather x1, waiting for transfers between devices, on_device(): lax.all_gather(pool_back, ('sp', 'fs'), axis=1, tiled=True)  83.4 us
    all_gather x1, waiting for transfers between devices, on_device(): lax.all_gather(retention_back, ('sp', 'fs'))  48.7 us
    all_gather x1, waiting for transfers between devices, on_device(): group_normed = lax.all_gather(normed, 'fs', axis=0, tiled=True)  47.3 us
    all_gather x1, waiting for transfers between devices, carried_in(): pieces = jax.tree.map(lambda part: lax.all_gather(part, axis), value)  41.1 us
    all_gather x1, waiting for transfers between devices, on_device(): lax.all_gather(quarters[2], 'sp', axis=0, tiled=True)  21.8 us
    all_gather x1, waiting for transfers between devices, on_device(): lax.all_gather(quarters[3], 'sp', axis=0, tiled=True)  20.7 us
    dot_general x4, matrix products, on_device(): jnp.dot(group_normed, piece_w, preferred_element_type=jnp.float32)  15.7 us
    all_gather x1, blocking collectives, on_device(): whole_start = lax.all_gather(start_state, 'sp', axis=2, tiled=True)[0]  14.9 us
  transfers between devices with their start and end apart: 14, of which 9 were waited for; matrix products, arithmetic and copies ran while one was open for 10% of the time, Pallas kernels for 0%

profile of v1, /device:TPU:0, one launch (start us, length us, event | category | flops | bytes accessed | tf_op | source)
XLA Modules:
  0.0 421.5 jit_solution(11480839695405417434)
XLA Ops:
  7.7 10.7 %all_to_all.137 = bf16[256,4,128]{0,2,1:T(8,128)(2,1)S(1)} all-to-all(bf16[256,4,128]{0,2,1:T(8,128)(2,1)S(1)} %bitcast.107), channel_id=1, replica_groups=mesh['sp'=4,'fs'=4,'tp'=2] {'fs'}, dimensions={1} | all-to-all | bytes 524288 | tf_op jit(solution)/shard_map/all_to_all | solution.py:140
  23.7 8.1 %all_to_all.138 = bf16[256,4,128]{0,2,1:T(8,128)(2,1)S(1)} all-to-all(bf16[256,4,128]{0,2,1:T(8,128)(2,1)S(1)} %bitcast.108), channel_id=1, replica_groups=mesh['sp'=4,'fs'=4,'tp'=2] {'fs'}, dimensions={1} | all-to-all | bytes 524288 | tf_op jit(solution)/shard_map/all_to_all | solution.py:141
  32.9 8.1 %all_to_all.139 = bf16[256,4,128]{0,2,1:T(8,128)(2,1)S(1)} all-to-all(bf16[256,4,128]{0,2,1:T(8,128)(2,1)S(1)} %bitcast.109), channel_id=1, replica_groups=mesh['sp'=4,'fs'=4,'tp'=2] {'fs'}, dimensions={1} | all-to-all | bytes 524288 | tf_op jit(solution)/shard_map/all_to_all | solution.py:142
  42.1 8.1 %all_to_all.140 = bf16[256,4,128]{0,2,1:T(8,128)(2,1)S(1)} all-to-all(bf16[256,4,128]{0,2,1:T(8,128)(2,1)S(1)} %bitcast.110), channel_id=1, replica_groups=mesh['sp'=4,'fs'=4,'tp'=2] {'fs'}, dimensions={1} | all-to-all | bytes 524288 | tf_op jit(solution)/shard_map/all_to_all | solution.py:139
  53.7 47.3 %all-gather.12.cloned.1.call-done = bf16[512,4096]{1,0:T(8,128)(2,1)} async-done(((bf16[128,4096]{1,0:T(8,128)(2,1)}), bf16[512,4096]{1,0:T(8,128)(2,1)}) %all-gather.12.cloned.1.call-update) | async-done | bytes 4194320 | tf_op jit(solution)/shard_map/all_gather | solution.py:137
  101.0 3.7 convolution_convert_fusion.1
  108.8 21.8 %all-gather.20.cloned.1.call-done = bf16[4096,128]{1,0:T(8,128)(2,1)} async-done(((bf16[1024,128]{1,0:T(8,128)(2,1)}), bf16[4096,128]{1,0:T(8,128)(2,1)}) %all-gather.20.cloned.1.call-update) | async-done | bytes 1048592 | tf_op jit(solution)/shard_map/all_gather | solution.py:147
  130.6 3.7 convolution_convert_fusion
  135.1 3.6 all-to-all-start.7
  138.8 20.7 %all-gather.16.cloned.1.call-done = bf16[4096,128]{1,0:T(8,128)(2,1)} async-done(((bf16[1024,128]{1,0:T(8,128)(2,1)}), bf16[4096,128]{1,0:T(8,128)(2,1)}) %all-gather.16.cloned.1.call-update) | async-done | bytes 1048592 | tf_op jit(solution)/shard_map/all_gather | solution.py:148
  159.4 4.4 %convolution_convert_fusion.2 = bf16[512,128]{1,0:T(8,128)(2,1)} fusion(bf16[512,4096]{1,0:T(8,128)(2,1)} %all-gather.12.cloned.1.call-done, bf16[4096,128]{1,0:T(8,128)(2,1)} %all-gather.16.cloned.1.call-done), kind=kOutput, calls=%fused_computation.19 | convolution fusion | flops 536936448 | bytes 5373952 | tf_op jit(solution)/shard_map/dot_general | solution.py:151
  163.8 3.8 all-to-all-start.3
  168.1 4.5 %all-to-all-done.3 = bf16[4,128,128]{2,1,0:T(8,128)(2,1)S(1)} async-done(((bf16[4,128,128]{2,1,0:T(8,128)(2,1)}), bf16[4,128,128]{2,1,0:T(8,128)(2,1)S(1)}, u32[]{:S(2)}, u32[]{:S(2)}) %all-to-all-start.3) | async-done | bytes 131104 | tf_op jit(solution)/shard_map/all_to_all | solution.py:156
  174.9 10.7 %all-reduce = f32[8]{0:T(128)S(1)} all-reduce(f32[8]{0:T(128)S(1)} %get-tuple-element.181), channel_id=2, replica_groups=mesh['sp'=4,'fs'=4,'tp'=2] {'sp'}, use_global_device_ids=true, to_apply=%add | all-reduce | flops 8 | bytes 64
  186.5 14.9 %all_gather.48 = f32[1,2,256,256]{3,2,1,0:T(8,128)S(1)} all-gather(f32[1,2,64,256]{3,2,1,0:T(8,128)S(1)} %copy-done.4), channel_id=1, replica_groups=mesh['sp'=4,'fs'=4,'tp'=2] {'sp'}, dimensions={2}, use_global_device_ids=true | all-gather | bytes 655360 | tf_op jit(solution)/shard_map/all_gather | solution.py:193
  201.4 3.8 convolution_convert_fusion.3
  210.7 3.6 all-to-all-done.1
  219.5 48.7 %all-gather.26.cloned.1.call-done = bf16[8192,256]{1,0:T(8,128)(2,1)} async-done(((bf16[512,256]{1,0:T(8,128)(2,1)}), bf16[8192,256]{1,0:T(8,128)(2,1)}) %all-gather.26.cloned.1.call-update) | async-done | bytes 4194320 | tf_op jit(solution)/shard_map/all_gather | solution.py:210
  268.2 4.8 %copy.85 = bf16[16,64,8,256]{3,2,0,1:T(8,128)(2,1)} copy(bf16[16,64,8,256]{3,2,1,0:T(8,128)(2,1)} %bitcast.90) | data formatting | bytes 8388608 | tf_op jit(solution)/shard_map/reshape | solution.py:210
  273.0 41.1 %all-gather.24.cloned.1.call-done = f32[8,256,256]{2,1,0:T(8,128)} async-done(((f32[2,256,256]{2,1,0:T(8,128)}), f32[8,256,256]{2,1,0:T(8,128)}) %all-gather.24.cloned.1.call-update) | async-done | bytes 2097168 | tf_op jit(solution)/shard_map/all_gather | solution.py:27
  314.1 3.6 while.9
  319.0 83.4 %all-gather.22.cloned.1.call-done = bf16[512,4096]{1,0:T(8,128)(2,1)} async-done(((bf16[512,256]{1,0:T(8,128)(2,1)}), bf16[512,4096]{1,0:T(8,128)(2,1)}) %all-gather.22.cloned.1.call-update) | async-done | bytes 4194320 | tf_op jit(solution)/shard_map/all_gather | solution.py:209
  402.4 5.8 %fusion.5 = bf16[128,4096]{1,0:T(8,128)(2,1)} fusion(bf16[512,4096]{1,0:T(8,128)(2,1)} %bitcast.91, bf16[512,4096]{1,0:T(8,128)(2,1)} %all-gather.22.cloned.1.call-done, bf16[128,512]{1,0:T(8,128)(2,1)S(1)} %copy.80, bf16[128,512]{1,0:T(8,128)(2,1)S(1)} %fusion.15), kind=kOutput, calls=%fused_computation.7 | convolution fusion | flops 1091567616 | bytes 9699328 | tf_op jit(solution)/shard_map/dot_general | solution.py:215
  408.3 6.7 %reduce-scatter.2.cloned.1.call-done = bf16[64,4096]{1,0:T(8,128)(2,1)} async-done(((bf16[128,4096]{1,0:T(8,128)(2,1)}), bf16[64,4096]{1,0:T(8,128)(2,1)}) %reduce-scatter.2.cloned.1.call-update) | async-done | bytes 524304 | tf_op jit(solution)/shard_map/reduce_scatter | solution.py:214
  (108 shorter events, 35.1 us)
Async XLA Ops:
  6.5 212.4 %copy-start = (bf16[4,256,256]{2,1,0:T(8,128)(2,1)S(1)}, bf16[4,256,256]{2,1,0:T(8,128)(2,1)}, u32[]{:S(2)}) copy-start(bf16[4,256,256]{2,1,0:T(8,128)(2,1)} %param.23) | copy-start | bytes 1572868
  6.5 17.1 %copy-start.1 = (bf16[256,512]{1,0:T(8,128)(2,1)S(1)}, bf16[256,512]{1,0:T(8,128)(2,1)}, u32[]{:S(2)}) copy-start(bf16[256,512]{1,0:T(8,128)(2,1)} %param.21) | copy-start | bytes 786436
  6.5 26.2 %copy-start.2 = (bf16[256,512]{1,0:T(8,128)(2,1)S(1)}, bf16[256,512]{1,0:T(8,128)(2,1)}, u32[]{:S(2)}) copy-start(bf16[256,512]{1,0:T(8,128)(2,1)} %param.22) | copy-start | bytes 786436
  6.5 47.1 %all-gather.18.cloned.1.call-start = ((), (), s32[]{:S(2)}) async-start(), calls=%async_computation.12 | async-start | bytes 1310720 | tf_op jit(solution)/shard_map/all_gather | solution.py:146
  19.3 22.7 %copy-start.3 = (bf16[256,512]{1,0:T(8,128)(2,1)S(1)}, bf16[256,512]{1,0:T(8,128)(2,1)}, u32[]{:S(2)}) copy-start(bf16[256,512]{1,0:T(8,128)(2,1)} %param.19) | copy-start | bytes 786436
  19.3 81.7 %all-gather.12.cloned.1.call-start = ((), (), s32[]{:S(2)}) async-start(), calls=%async_computation.9 | async-start | bytes 5242880 | tf_op jit(solution)/shard_map/all_gather | solution.py:137
  20.9 30.8 %copy-start.8 = (u32[32]{0:T(128)S(1)}, u32[32]{0:T(128)}, u32[]{:S(2)}) copy-start(u32[32]{0:T(128)} %constant.104) | copy-start | bytes 388
  20.9 32.2 %copy-start.5 = (f32[2]{0:T(128)S(1)}, f32[2]{0:T(128)}, u32[]{:S(2)}) copy-start(f32[2]{0:T(128)} %param.25) | copy-start | bytes 28
  23.5 107.0 %all-gather.20.cloned.1.call-start = ((), (), s32[]{:S(2)}) async-start(), calls=%async_computation.13 | async-start | bytes 1310720 | tf_op jit(solution)/shard_map/all_gather | solution.py:147
  32.7 126.7 %all-gather.16.cloned.1.call-start = ((), (), s32[]{:S(2)}) async-start(), calls=%async_computation.11 | async-start | bytes 1310720 | tf_op jit(solution)/shard_map/all_gather | solution.py:148
  41.9 159.5 %all-gather.14.cloned.1.call-start = ((), (), s32[]{:S(2)}) async-start(), calls=%async_computation.10 | async-start | bytes 1310720 | tf_op jit(solution)/shard_map/all_gather | solution.py:145
  51.1 217.2 %all-gather.26.cloned.1.call-start = ((), (), s32[]{:S(2)}) async-start(), calls=%async_computation.17 | async-start | bytes 4456448 | tf_op jit(solution)/shard_map/all_gather | solution.py:210
  105.5 29.6 %all-to-all-start.5 = ((bf16[4,128,128]{1,2,0:T(8,128)(2,1)}), bf16[4,128,128]{1,2,0:T(8,128)(2,1)S(1)}, u32[]{:S(2)}, u32[]{:S(2)}) async-start(bf16[4,128,128]{1,2,0:T(8,128)(2,1)} %copy.63), calls=%async_computation.5 | async-start | bytes 262144 | tf_op jit(solution)/shard_map/all_to_all | solution.py:156
  135.1 28.7 %all-to-all-start.7 = ((bf16[4,128,128]{1,2,0:T(8,128)(2,1)}), bf16[4,128,128]{1,2,0:T(8,128)(2,1)S(1)}, u32[]{:S(2)}, u32[]{:S(2)}) async-start(bf16[4,128,128]{1,2,0:T(8,128)(2,1)} %copy.68), calls=%async_computation.7 | async-start | bytes 262144 | tf_op jit(solution)/shard_map/all_to_all | solution.py:156
  163.8 21.9 %copy-start.7 = (f32[1024]{0:T(1024)S(1)}, f32[1024]{0:T(1024)}, u32[]{:S(2)}) copy-start(f32[1024]{0:T(1024)} %param.24) | copy-start | bytes 12292
  163.8 22.0 %copy-start.6 = (s32[4]{0:T(128)S(1)}, s32[4]{0:T(128)}, u32[]{:S(2)}) copy-start(s32[4]{0:T(128)} %constant.99.clone) | copy-start | bytes 52
  163.8 22.7 %copy-start.4 = (f32[1,2,64,256]{3,2,1,0:T(8,128)S(1)}, f32[1,2,64,256]{3,2,1,0:T(8,128)}, u32[]{:S(2)}) copy-start(f32[1,2,64,256]{3,2,1,0:T(8,128)} %param.26) | copy-start | bytes 393220
  163.8 8.8 %all-to-all-start.3 = ((bf16[4,128,128]{2,1,0:T(8,128)(2,1)}), bf16[4,128,128]{2,1,0:T(8,128)(2,1)S(1)}, u32[]{:S(2)}, u32[]{:S(2)}) async-start(bf16[4,128,128]{2,1,0:T(8,128)(2,1)} %bitcast.22), calls=%async_computation.3 | async-start | bytes 262144 | tf_op jit(solution)/shard_map/all_to_all | solution.py:156
  167.6 146.5 %all-gather.24.cloned.1.call-start = ((), (), s32[]{:S(2)}) async-start(), calls=%async_computation.16 | async-start | bytes 2621440 | tf_op jit(solution)/shard_map/all_gather | solution.py:27
  174.2 228.3 %all-gather.22.cloned.1.call-start = ((), (), s32[]{:S(2)}) async-start(), calls=%async_computation.14 | async-start | bytes 4456448 | tf_op jit(solution)/shard_map/all_gather | solution.py:209
  206.0 8.3 %all-to-all-start.1 = ((bf16[4,128,128]{1,2,0:T(8,128)(2,1)}), bf16[4,128,128]{1,2,0:T(8,128)(2,1)S(1)}, u32[]{:S(2)}, u32[]{:S(2)}) async-start(bf16[4,128,128]{1,2,0:T(8,128)(2,1)} %copy.55), calls=%async_computation.1 | async-start | bytes 262144 | tf_op jit(solution)/shard_map/all_to_all | solution.py:156
  209.3 205.7 %reduce-scatter.2.cloned.1.call-start = ((), (), s32[]{:S(2)}) async-start(), calls=%async_computation.15 | async-start | bytes 1572864 | tf_op jit(solution)/shard_map/reduce_scatter | solution.py:214
  214.5 2.8 collective-permute-start
Sparse Core Ops, SparseCore 0:
  19.4 27.6 all-gather.17
  49.0 51.9 all-gather.11
  102.6 27.9 all-gather.19
  132.0 27.3 all-gather.15
  160.8 29.0 all-gather.13
  192.5 75.6 all-gather.25
  269.8 44.2 all-gather.23
  316.8 85.5 all-gather.21
  408.4 6.5 reduce-scatter.1
